TPU v7x, 128 devices: a whole 4x4x4 slice. The times are simulated.
128 devices in a mesh: fs: 16 (over z, y), tp: 8 (over x, core).
Axes of the slice: x: 4, y: 4, z: 4, core: 2. Of those that a mesh axis runs over, the one named last changes fastest.
Arguments:
- tokens: bfloat16 [16384, 2048], P('fs', 'tp'), may hold values from -6 to 6
- norm_gain: float32 [2048], P('fs'), may hold values from 0.1 to 1.9
- up_master: float32 [2048, 8192], P('fs', 'tp'), may hold values from -0.125 to 0.125
- down_master: float32 [2048, 8192], P('fs', 'tp'), may hold values from -0.0625 to 0.0625
Outputs:
- up_weights: bfloat16 [2048, 8192], P(None, 'tp')
- down_weights: bfloat16 [8192, 2048], P('tp')
- mlp_out: bfloat16 [16384, 2048], P('fs', 'tp')
All inputs are finite; a program needn't handle non-finite values.
Results may differ from a plain program's by a relative error of at most 0.014.
Values may be sent and summed in bfloat16 or wider, within the bound.
A program may use at most 128 MiB of HBM per device.

v0:
```python
import jax
import jax.numpy as jnp
from jax import lax
from jax.sharding import PartitionSpec as P

norm_floor = 1e-06


def side_by_side(arrays, axis, dim, along):
    ends, at = ([], 0)
    for a in arrays[:-1]:
        at += a.shape[along]
        ends.append(at)
    both = jnp.concatenate(arrays, axis=along)
    return tuple(jnp.split(lax.all_gather(both, axis, axis=dim, tiled=True), ends, axis=along))


def on_device(tokens, norm_gain, up_master, down_master):
    up_local = (norm_gain[:, None] * up_master).astype(jnp.bfloat16)
    down_local = down_master.astype(jnp.bfloat16)
    gathered = lax.all_gather(tokens, "tp", axis=1, tiled=True)
    widened = gathered.astype(jnp.float32)
    normed = (
        widened * lax.rsqrt(jnp.mean(widened * widened, axis=-1, keepdims=True) + norm_floor)
    ).astype(jnp.bfloat16)
    up_whole, down_whole = side_by_side((up_local, down_local), "fs", 0, 1)
    preact = jnp.dot(normed, up_whole, preferred_element_type=jnp.float32)
    hidden = jnp.square(jax.nn.relu(preact)).astype(jnp.bfloat16)
    partial_value = jnp.einsum("tf,df->td", hidden, down_whole, preferred_element_type=jnp.float32)
    summed = lax.psum_scatter(
        partial_value.astype(jnp.bfloat16), "tp", scatter_dimension=1, tiled=True
    )
    return (up_whole, jnp.transpose(down_whole), summed)


def solution(mesh):
    in_specs = (P("fs", "tp"), P("fs"), P("fs", "tp"), P("fs", "tp"))
    out_specs = (P(None, "tp"), P("tp", None), P("fs", "tp"))
    return jax.shard_map(
        on_device, mesh=mesh, in_specs=in_specs, out_specs=out_specs, check_vma=False
    )
```

profile of v0, /device:TPU:0, one launch (start us, length us, event | category | flops | bytes accessed | tf_op | source)
XLA Modules:
  0.0 186.4 jit_solution(12943971067631530127)
XLA Ops:
  7.2 0.0 all-gather.5.cloned.1.call-start
  7.2 0.7 all-gather.5.cloned.1.call-update
  7.9 0.0 all-gather.3.cloned.1.call-start
  7.9 1.2 copy.7
  9.2 1.2 copy.8
  10.4 0.7 multiply_convert_fusion.2
  11.1 0.8 pad_maximum_fusion
  11.9 0.0 all-gather.3.cloned.1.call-update
  12.0 0.0 reduce-scatter.2.cloned.1.call-start
  12.0 35.6 %all-gather.5.cloned.1.call-done = bf16[1024,2048]{1,0:T(8,128)(2,1)} async-done(((bf16[1024,256]{1,0:T(8,128)(2,1)}), bf16[1024,2048]{1,0:T(8,128)(2,1)}) %all-gather.5.cloned.1.call-update) | async-done | bytes 4194320 | tf_op jit(solution)/shard_map/all_gather | solution.py:21
  47.7 3.1 %fusion = f32[1024]{0:T(1024)S(1)} fusion(bf16[1024,2048]{1,0:T(8,128)(2,1)} %all-gather.5.cloned.1.call-done), kind=kLoop, calls=%fused_computation.2 | loop fusion | flops 6290432 | bytes 4198400 | tf_op jit(solution)/shard_map/reduce_sum | solution.py:24
  50.7 78.0 %all-gather.3.cloned.1.call-done = bf16[2048,2048]{0,1:T(8,128)(2,1)} async-done(((bf16[128,2048]{0,1:T(8,128)(2,1)}), bf16[2048,2048]{0,1:T(8,128)(2,1)}) %all-gather.3.cloned.1.call-update) | async-done | bytes 8388624 | tf_op jit(solution)/shard_map/all_gather | solution.py:15
  128.7 0.0 copy-start
  128.7 7.7 %fusion.2 = f32[1024,1024]{1,0:T(8,128)S(1)} fusion(bf16[1024,2048]{1,0:T(8,128)(2,1)} %all-gather.5.cloned.1.call-done, f32[1024]{0:T(1024)S(1)} %add_rsqrt_fusion, bf16[2048,2048]{0,1:T(8,128)(2,1)} %all-gather.3.cloned.1.call-done), kind=kOutput, calls=%fused_computation.4 | convolution fusion | flops 4301258752 | bytes 12587008 | tf_op jit(solution)/shard_map/dot_general | solution.py:27
  136.5 0.0 copy-done
  136.5 6.1 %convolution_convert_fusion = bf16[1024,2048]{1,0:T(8,128)(2,1)} fusion(bf16[2048,2048]{0,1:T(8,128)(2,1)S(1)} %copy-done, f32[1024,1024]{1,0:T(8,128)S(1)} %fusion.2), kind=kOutput, calls=%fused_computation.7 | convolution fusion | flops 4300210176 | bytes 12582912 | tf_op jit(solution)/shard_map/tf,df->td/dot_general | solution.py:29
  142.6 0.0 reduce-scatter.2.cloned.1.call-update
  142.6 6.2 %slice_bitcast_fusion = (bf16[1024,2048]{1,0:T(8,128)(2,1)}, bf16[2048,1024]{0,1:T(8,128)(2,1)}) fusion(bf16[2048,2048]{0,1:T(8,128)(2,1)} %all-gather.3.cloned.1.call-done), kind=kLoop, calls=%fused_computation.9 | loop fusion | bytes 16777216 | tf_op jit(solution)/shard_map/transpose | solution.py:33
  148.7 6.4 %copy.9 = bf16[2048,1024]{1,0:T(8,128)(2,1)} copy(bf16[2048,1024]{0,1:T(8,128)(2,1)} %get-tuple-element.7) | data formatting | bytes 8388608
  155.2 24.7 %reduce-scatter.2.cloned.1.call-done = bf16[1024,256]{1,0:T(8,128)(2,1)} async-done(((bf16[1024,2048]{1,0:T(8,128)(2,1)}), bf16[1024,256]{1,0:T(8,128)(2,1)}) %reduce-scatter.2.cloned.1.call-update) | async-done | bytes 524304 | tf_op jit(solution)/shard_map/reduce_scatter | solution.py:30
  (1 shorter events, 0.0 us)
Async XLA Ops:
  7.2 40.5 %all-gather.5.cloned.1.call-start = ((), (), s32[]{:S(2)}) async-start(), calls=%async_computation.2 | async-start | bytes 4718592 | tf_op jit(solution)/shard_map/all_gather | solution.py:21
  7.9 120.8 %all-gather.3.cloned.1.call-start = ((), (), s32[]{:S(2)}) async-start(), calls=%async_computation.1 | async-start | bytes 8912896 | tf_op jit(solution)/shard_map/all_gather | solution.py:15
  12.0 167.9 %reduce-scatter.2.cloned.1.call-start = ((), (), s32[]{:S(2)}) async-start(), calls=%async_computation.3 | async-start | bytes 4718592 | tf_op jit(solution)/shard_map/reduce_scatter | solution.py:30
  128.7 7.8 %copy-start = (bf16[2048,2048]{0,1:T(8,128)(2,1)S(1)}, bf16[2048,2048]{0,1:T(8,128)(2,1)}, u32[]{:S(2)}) copy-start(bf16[2048,2048]{0,1:T(8,128)(2,1)} %all-gather.3.cloned.1.call-done) | copy-start | bytes 25165828
Sparse Core Ops, SparseCore 0:
  9.7 37.9 all-gather.4
  50.3 78.3 all-gather.2
  142.7 37.0 reduce-scatter.1
where the time goes:
time: 187 us; the launch traced here: 186 us
  waiting for transfers between devices  139 us (74%)
  local copies, waits for them, and re-layouts  15 us (8%)
  matrix products  13.8 us (7%)
  between operations  13.8 us (7%)
  other arithmetic  4.6 us (2%)
    all_gather x1, waiting for transfers between devices, side_by_side(): lax.all_gather(both, axis, axis=dim, tiled=True)  78 us
    all_gather x1, waiting for transfers between devices, on_device(): gathered = lax.all_gather(tokens, 'tp', axis=1, tiled=True)  35.6 us
    reduce_scatter x1, waiting for transfers between devices, on_device(): lax.psum_scatter(partial_value.astype(jnp.bfloat16), 'tp', scatter_dimens...  24.7 us
    unnamed x5, local copies, waits for them, and re-layouts  8.86 us
    dot_general x1, matrix products, on_device(): preact = jnp.dot(normed, up_whole, preferred_element_type=jnp.float32)  7.74 us
    transpose x1, local copies, waits for them, and re-layouts, on_device(): return (up_whole, jnp.transpose(down_whole), summed)  6.15 us
    dot_general x1, matrix products, on_device(): jnp.einsum('tf,df->td', hidden, down_whole, preferred_element_type=jnp.fl...  6.09 us
  transfers between devices with their start and end apart: 3, of which 3 were waited for; matrix products, arithmetic and copies ran while one was open for 11% of the time, Pallas kernels for 0%

commit v1 on v0

--- a/solution.py
+++ b/solution.py
@@ -18,7 +18,12 @@
 def on_device(tokens, norm_gain, up_master, down_master):
     up_local = (norm_gain[:, None] * up_master).astype(jnp.bfloat16)
     down_local = down_master.astype(jnp.bfloat16)
-    gathered = lax.all_gather(tokens, "tp", axis=1, tiled=True)
+    ring = [tokens]
+    for hop in range(7):
+        ring.append(lax.ppermute(ring[-1], "tp", [(dev, (dev + 1) % 8) for dev in range(8)]))
+    gathered = jnp.roll(
+        jnp.concatenate(ring[::-1], axis=1), (lax.axis_index("tp") + 1) * ring[0].shape[1], axis=1
+    )
     widened = gathered.astype(jnp.float32)
     normed = (
         widened * lax.rsqrt(jnp.mean(widened * widened, axis=-1, keepdims=True) + norm_floor)

time: 187 us -> 150 us (0.80)
  waiting for transfers between devices: 139 us -> 95.2 us
  local copies, waits for them, and re-layouts: 15 us -> 23.6 us
  other arithmetic: 4.6 us -> 2.41 us
    all_gather x1, waiting for transfers between devices: 78 us -> 1.06 us  [side_by_side(): lax.all_gather(both, axis, axis=dim, tiled=True)]
    ppermute x0 -> x7, waiting for transfers between devices: none -> 69.3 us  [on_device(): lax.ppermute(ring[-1], 'tp', [(dev, (dev + 1) % 8) for dev in range(8)])]
    all_gather x1 -> x0, waiting for transfers between devices: 35.6 us -> none  [on_device(): gathered = lax.all_gather(tokens, 'tp', axis=1, tiled=True)]
    unnamed x5 -> x24, local copies, waits for them, and re-layouts: 8.86 us -> 17.4 us
    reduce_sum x1, other arithmetic: 3.07 us -> 0.88 us  [on_device(): jnp.mean(widened * widened, axis=-1, keepdims=True) + norm_floor]
  transfers between devices with their start and end apart: 3 -> 9, of which waited for: 3 -> 9; matrix products, arithmetic and copies ran while one was open for 11% -> 13% of each run, Pallas kernels for 0% -> 0%
where the time goes in v1:
time: 150 us; the launch traced here: 149 us
  waiting for transfers between devices  95.2 us (63%)
  local copies, waits for them, and re-layouts  23.6 us (16%)
  between operations  14.2 us (9%)
  matrix products  13.8 us (9%)
  other arithmetic  2.41 us (2%)
    ppermute x7, waiting for transfers between devices, on_device(): lax.ppermute(ring[-1], 'tp', [(dev, (dev + 1) % 8) for dev in range(8)])  69.3 us
    reduce_scatter x1, waiting for transfers between devices, on_device(): lax.psum_scatter(partial_value.astype(jnp.bfloat16), 'tp', scatter_dimens...  24.8 us
    unnamed x24, local copies, waits for them, and re-layouts  17.4 us
    dot_general x1, matrix products, on_device(): preact = jnp.dot(normed, up_whole, preferred_element_type=jnp.float32)  7.74 us
    transpose x1, local copies, waits for them, and re-layouts, on_device(): return (up_whole, jnp.transpose(down_whole), summed)  6.13 us
    dot_general x1, matrix products, on_device(): jnp.einsum('tf,df->td', hidden, down_whole, preferred_element_type=jnp.fl...  6.09 us
  transfers between devices with their start and end apart: 9, of which 9 were waited for; matrix products, arithmetic and copies ran while one was open for 13% of the time, Pallas kernels for 0%

profile of v1, /device:TPU:0, one launch (start us, length us, event | category | flops | bytes accessed | tf_op | source)
XLA Modules:
  0.0 149.3 jit_solution(6531392363771260607)
XLA Ops:
  7.2 1.3 copy.7
  8.5 1.2 copy.8
  9.7 0.7 multiply_convert_fusion.2
  10.4 0.8 pad_maximum_fusion
  11.4 10.0 %collective-permute-done = bf16[1024,256]{1,0:T(8,128)(2,1)S(1)} collective-permute-done((bf16[1024,256]{1,0:T(8,128)(2,1)}, bf16[1024,256]{1,0:T(8,128)(2,1)S(1)}, u32[]{:S(2)}, u32[]{:S(2)}) %collective-permute-start) | collective-permute-done | bytes 524320 | tf_op jit(solution)/shard_map/ppermute | solution.py:23
  21.4 9.8 %collective-permute-done.1 = bf16[1024,256]{1,0:T(8,128)(2,1)S(1)} collective-permute-done((bf16[1024,256]{1,0:T(8,128)(2,1)S(1)}, bf16[1024,256]{1,0:T(8,128)(2,1)S(1)}, u32[]{:S(2)}, u32[]{:S(2)}) %collective-permute-start.1) | collective-permute-done | bytes 524320 | tf_op jit(solution)/shard_map/ppermute | solution.py:23
  31.2 9.8 %collective-permute-done.2 = bf16[1024,256]{1,0:T(8,128)(2,1)S(1)} collective-permute-done((bf16[1024,256]{1,0:T(8,128)(2,1)S(1)}, bf16[1024,256]{1,0:T(8,128)(2,1)S(1)}, u32[]{:S(2)}, u32[]{:S(2)}) %collective-permute-start.2) | collective-permute-done | bytes 524320 | tf_op jit(solution)/shard_map/ppermute | solution.py:23
  41.0 9.8 %collective-permute-done.3 = bf16[1024,256]{1,0:T(8,128)(2,1)S(1)} collective-permute-done((bf16[1024,256]{1,0:T(8,128)(2,1)S(1)}, bf16[1024,256]{1,0:T(8,128)(2,1)S(1)}, u32[]{:S(2)}, u32[]{:S(2)}) %collective-permute-start.3) | collective-permute-done | bytes 524320 | tf_op jit(solution)/shard_map/ppermute | solution.py:23
  50.8 9.8 %collective-permute-done.4 = bf16[1024,256]{1,0:T(8,128)(2,1)S(1)} collective-permute-done((bf16[1024,256]{1,0:T(8,128)(2,1)S(1)}, bf16[1024,256]{1,0:T(8,128)(2,1)S(1)}, u32[]{:S(2)}, u32[]{:S(2)}) %collective-permute-start.4) | collective-permute-done | bytes 524320 | tf_op jit(solution)/shard_map/ppermute | solution.py:23
  60.6 9.9 %collective-permute-done.5 = bf16[1024,256]{1,0:T(8,128)(2,1)} collective-permute-done((bf16[1024,256]{1,0:T(8,128)(2,1)S(1)}, bf16[1024,256]{1,0:T(8,128)(2,1)}, u32[]{:S(2)}, u32[]{:S(2)}) %collective-permute-start.5) | collective-permute-done | bytes 524320 | tf_op jit(solution)/shard_map/ppermute | solution.py:23
  70.6 10.1 %collective-permute-done.6 = bf16[1024,256]{1,0:T(8,128)(2,1)} collective-permute-done((bf16[1024,256]{1,0:T(8,128)(2,1)}, bf16[1024,256]{1,0:T(8,128)(2,1)}, u32[]{:S(2)}, u32[]{:S(2)}) %collective-permute-start.6) | collective-permute-done | bytes 524320 | tf_op jit(solution)/shard_map/ppermute | solution.py:23
  80.7 1.1 constant_dynamic-update-slice_fusion.15
  81.8 1.1 constant_dynamic-update-slice_fusion.14
  83.0 0.1 constant_dynamic-update-slice_fusion.12
  83.1 0.1 constant_dynamic-update-slice_fusion.11
  83.2 0.1 constant_dynamic-update-slice_fusion.10
  83.3 0.1 constant_dynamic-update-slice_fusion.9
  83.4 1.1 constant_dynamic-update-slice_fusion.7
  84.5 1.1 constant_dynamic-update-slice_fusion.6
  85.7 0.1 constant_dynamic-update-slice_fusion.4
  85.8 0.1 constant_dynamic-update-slice_fusion.3
  85.9 0.1 constant_dynamic-update-slice_fusion.2
  86.0 0.1 constant_dynamic-update-slice_fusion.1
  86.0 0.1 constant_dynamic-update-slice_fusion
  86.1 3.2 %copy-done.1 = bf16[1024,4096]{1,0:T(8,128)(2,1)} copy-done((bf16[1024,4096]{1,0:T(8,128)(2,1)}, bf16[1024,4096]{1,0:T(8,128)(2,1)S(1)}, u32[]{:S(2)}) %copy-start.1) | copy-done | bytes 8388632
  89.3 0.9 fusion
  90.2 1.1 all-gather.2.cloned.1.call-done
  91.3 7.7 %fusion.2 = f32[1024,1024]{1,0:T(8,128)S(1)} fusion(f32[1024]{0:T(1024)S(1)} %add_rsqrt_fusion, bf16[1024,4096]{1,0:T(8,128)(2,1)} %copy-done.1, s32[]{:T(128)S(6)} %select_n.14, bf16[2048,2048]{0,1:T(8,128)(2,1)} %all-gather.2.cloned.1.call-done), kind=kOutput, calls=%fused_computation.4 | convolution fusion | flops 4301258752 | bytes 12587012 | tf_op jit(solution)/shard_map/dot_general | solution.py:32
  99.1 6.1 %convolution_convert_fusion = bf16[1024,2048]{1,0:T(8,128)(2,1)} fusion(bf16[2048,2048]{0,1:T(8,128)(2,1)S(1)} %copy-done, f32[1024,1024]{1,0:T(8,128)S(1)} %fusion.2), kind=kOutput, calls=%fused_computation.7 | convolution fusion | flops 4300210176 | bytes 12582912 | tf_op jit(solution)/shard_map/tf,df->td/dot_general | solution.py:34
  105.2 6.1 %slice_bitcast_fusion = (bf16[1024,2048]{1,0:T(8,128)(2,1)}, bf16[2048,1024]{0,1:T(8,128)(2,1)}) fusion(bf16[2048,2048]{0,1:T(8,128)(2,1)} %all-gather.2.cloned.1.call-done), kind=kLoop, calls=%fused_computation.9 | loop fusion | bytes 16777216 | tf_op jit(solution)/shard_map/transpose | solution.py:38
  111.3 6.4 %copy.9 = bf16[2048,1024]{1,0:T(8,128)(2,1)} copy(bf16[2048,1024]{0,1:T(8,128)(2,1)} %get-tuple-element.7) | data formatting | bytes 8388608
  117.7 24.8 %reduce-scatter.2.cloned.1.call-done = bf16[1024,256]{1,0:T(8,128)(2,1)} async-done(((bf16[1024,2048]{1,0:T(8,128)(2,1)}), bf16[1024,256]{1,0:T(8,128)(2,1)}) %reduce-scatter.2.cloned.1.call-update) | async-done | bytes 524304 | tf_op jit(solution)/shard_map/reduce_scatter | solution.py:35
  (20 shorter events, 0.4 us)
Async XLA Ops:
  7.2 76.2 %copy-start.2 = (bf16[1024,256]{1,0:T(8,128)(2,1)S(1)}, bf16[1024,256]{1,0:T(8,128)(2,1)}, u32[]{:S(2)}) copy-start(bf16[1024,256]{1,0:T(8,128)(2,1)} %param.4) | copy-start | bytes 1572868
  7.2 84.1 %all-gather.2.cloned.1.call-start = ((), (), s32[]{:S(2)}) async-start(), calls=%async_computation.1 | async-start | bytes 8912896 | tf_op jit(solution)/shard_map/all_gather | solution.py:15
  11.3 131.2 %reduce-scatter.2.cloned.1.call-start = ((), (), s32[]{:S(2)}) async-start(), calls=%async_computation.2 | async-start | bytes 4718592 | tf_op jit(solution)/shard_map/reduce_scatter | solution.py:35
  11.3 10.0 %collective-permute-start = (bf16[1024,256]{1,0:T(8,128)(2,1)}, bf16[1024,256]{1,0:T(8,128)(2,1)S(1)}, u32[]{:S(2)}, u32[]{:S(2)}) collective-permute-start(bf16[1024,256]{1,0:T(8,128)(2,1)} %param.4), channel_id=1, source_target_pairs={{0,1},{1,2},{2,3},{3,4},{4,5},{5,6},{6,7},{7,0},{8,9},{9,10},{10,1... | collective-permute-start | bytes 1572872 | tf_op jit(solution)/shard_map/ppermute | solution.py:23
  21.4 9.8 %collective-permute-start.1 = (bf16[1024,256]{1,0:T(8,128)(2,1)S(1)}, bf16[1024,256]{1,0:T(8,128)(2,1)S(1)}, u32[]{:S(2)}, u32[]{:S(2)}) collective-permute-start(bf16[1024,256]{1,0:T(8,128)(2,1)S(1)} %collective-permute-done), channel_id=1, source_target_pairs={{0,1},{1,2},{2,3},{3,4},{4,5},{5,6},{6,7},{7,0},{8,9},{9,10},{10,1... | collective-permute-start | bytes 1572872 | tf_op jit(solution)/shard_map/ppermute | solution.py:23
  31.2 9.8 %collective-permute-start.2 = (bf16[1024,256]{1,0:T(8,128)(2,1)S(1)}, bf16[1024,256]{1,0:T(8,128)(2,1)S(1)}, u32[]{:S(2)}, u32[]{:S(2)}) collective-permute-start(bf16[1024,256]{1,0:T(8,128)(2,1)S(1)} %collective-permute-done.1), channel_id=1, source_target_pairs={{0,1},{1,2},{2,3},{3,4},{4,5},{5,6},{6,7},{7,0},{8,9},{9,10},{10,1... | collective-permute-start | bytes 1572872 | tf_op jit(solution)/shard_map/ppermute | solution.py:23
  41.0 9.8 %collective-permute-start.3 = (bf16[1024,256]{1,0:T(8,128)(2,1)S(1)}, bf16[1024,256]{1,0:T(8,128)(2,1)S(1)}, u32[]{:S(2)}, u32[]{:S(2)}) collective-permute-start(bf16[1024,256]{1,0:T(8,128)(2,1)S(1)} %collective-permute-done.2), channel_id=1, source_target_pairs={{0,1},{1,2},{2,3},{3,4},{4,5},{5,6},{6,7},{7,0},{8,9},{9,10},{10,1... | collective-permute-start | bytes 1572872 | tf_op jit(solution)/shard_map/ppermute | solution.py:23
  50.8 9.8 %collective-permute-start.4 = (bf16[1024,256]{1,0:T(8,128)(2,1)S(1)}, bf16[1024,256]{1,0:T(8,128)(2,1)S(1)}, u32[]{:S(2)}, u32[]{:S(2)}) collective-permute-start(bf16[1024,256]{1,0:T(8,128)(2,1)S(1)} %collective-permute-done.3), channel_id=1, source_target_pairs={{0,1},{1,2},{2,3},{3,4},{4,5},{5,6},{6,7},{7,0},{8,9},{9,10},{10,1... | collective-permute-start | bytes 1572872 | tf_op jit(solution)/shard_map/ppermute | solution.py:23
  60.6 9.9 %collective-permute-start.5 = (bf16[1024,256]{1,0:T(8,128)(2,1)S(1)}, bf16[1024,256]{1,0:T(8,128)(2,1)}, u32[]{:S(2)}, u32[]{:S(2)}) collective-permute-start(bf16[1024,256]{1,0:T(8,128)(2,1)S(1)} %collective-permute-done.4), channel_id=1, source_target_pairs={{0,1},{1,2},{2,3},{3,4},{4,5},{5,6},{6,7},{7,0},{8,9},{9,10},{10,1... | collective-permute-start | bytes 1572872 | tf_op jit(solution)/shard_map/ppermute | solution.py:23
  70.6 10.1 %collective-permute-start.6 = (bf16[1024,256]{1,0:T(8,128)(2,1)}, bf16[1024,256]{1,0:T(8,128)(2,1)}, u32[]{:S(2)}, u32[]{:S(2)}) collective-permute-start(bf16[1024,256]{1,0:T(8,128)(2,1)} %collective-permute-done.5), channel_id=1, source_target_pairs={{0,1},{1,2},{2,3},{3,4},{4,5},{5,6},{6,7},{7,0},{8,9},{9,10},{10,1... | collective-permute-start | bytes 1572872 | tf_op jit(solution)/shard_map/ppermute | solution.py:23
  86.1 3.2 %copy-start.1 = (bf16[1024,4096]{1,0:T(8,128)(2,1)}, bf16[1024,4096]{1,0:T(8,128)(2,1)S(1)}, u32[]{:S(2)}) copy-start(bf16[1024,4096]{1,0:T(8,128)(2,1)S(1)} %constant_dynamic-update-slice_fusion) | copy-start | bytes 25165828
  91.3 7.8 %copy-start = (bf16[2048,2048]{0,1:T(8,128)(2,1)S(1)}, bf16[2048,2048]{0,1:T(8,128)(2,1)}, u32[]{:S(2)}) copy-start(bf16[2048,2048]{0,1:T(8,128)(2,1)} %all-gather.2.cloned.1.call-done) | copy-start | bytes 25165828
Sparse Core Ops, SparseCore 0:
  11.4 79.8 all-gather.1
  105.3 37.1 reduce-scatter.1
